TPU v7x, 32 devices: a whole 2x2x4 slice. The times are simulated.
32 devices in a mesh: ep: 4 (over z), tp: 8 (over y, x, core).
Axes of the slice: x: 2, y: 2, z: 4, core: 2. Of those that a mesh axis runs over, the one named last changes fastest.
Arguments:
- tokens: bfloat16 [672, 2048], P('ep', 'tp'), may hold values from -540 to 540
- norm_gain: float32 [2048], P('tp'), may hold values from 0.1 to 1.9
- chosen: int32 [4, 504], P('ep'), may hold values from 0 to 671, as said below
- affinity: float32 [4, 504], P('ep'), may hold values from 0.1 to 1
- w_gate: bfloat16 [4, 2048, 8192], P('ep', None, 'tp'), may hold values from -0.125 to 0.125
- w_up: bfloat16 [4, 2048, 8192], P('ep', None, 'tp'), may hold values from -0.125 to 0.125
- w_down: bfloat16 [4, 8192, 2048], P('ep', 'tp'), may hold values from -0.0625 to 0.0625
Outputs:
- expert_mix: bfloat16 [672, 2048], P('ep', 'tp')
Inputs may be any that keep to these rules, and one draw needn't show every extreme that they name: `chosen`: each expert's 504 token numbers are distinct. Among one expert's choices at most 168 are tokens of one index of ep, and that bound is reached in every draw.
All inputs are finite; a program needn't handle non-finite values.
Results may differ from a plain program's by a relative error of at most 0.025.
Values may be sent and summed in bfloat16 or wider, within the bound.
A program may use at most 64 MiB of HBM per device.

v0:
```python
import functools

import jax
import jax.numpy as jnp
from jax import lax
from jax.experimental import pallas as pl
from jax.experimental.pallas import tpu as pltpu
from jax.sharding import PartitionSpec as P

MESH = pl.DeviceIdType.MESH
VMEM_BYTES = 67_043_328
LANES = 128
CHUNKS = 2
LAG = 1


def kernel(
    ep, tp, chunks,
    tok, gain, chosen, aff, wg_hbm, wu_hbm, wd_hbm,
    out,
    wg, wu, wd, full, normed, hidden, part, got1, got2, own, weighted,
    near, back, got_back, chosen_row, aff_row, aff_token, slot_row, slot_col,
    aff_col, gain_all, keep, w_sem, g_send, g_recv, z_send, z_recv, ag_send, ag_recv,
    r1_send, r1_recv, r2_send, r2_recv, b_send, b_recv,
):
    me = lax.axis_index("ep")
    t = lax.axis_index("tp")
    tok_dev, width = tok.shape
    rows = full.shape[1]
    d = wg.shape[0]
    count = chosen.shape[1]
    size = rows // chunks
    ff = wg.shape[1]
    f32, bf16 = jnp.float32, jnp.bfloat16

    def flip(m):
        index, bit = t, 1
        while bit <= m:
            if m & bit:
                index = index + bit - 2 * bit * ((t // bit) % 2)
            bit *= 2
        return index

    def cols(m):
        return pl.ds(pl.multiple_of(flip(m) * width, LANES), width)

    def remote(src, dst, send, recv, ep_to, tp_to):
        return pltpu.make_async_remote_copy(
            src_ref=src, dst_ref=dst, send_sem=send, recv_sem=recv,
            device_id=(ep_to, tp_to), device_id_type=MESH,
        )

    evens = [6, 2, 4]
    half = size // 2
    odds = [m + 1 for m in evens] + [1]
    order = list(range(chunks))
    weights = [
        pltpu.make_async_copy(h.at[0], v, w_sem.at[i])
        for i, (h, v) in enumerate(((wg_hbm, wg), (wu_hbm, wu), (wd_hbm, wd)))
    ]
    for copy in weights:
        copy.start()

    spare = ep * tok_dev - count
    need = [min(tok_dev, -(-(-(-(size * (c + 1) + spare) // ep)) // 16) * 16) for c in order]
    need[-1] = tok_dev
    least = [size * c // ep // 16 * 16 for c in order]
    done = [min(tok_dev, size * (c + 1) // ep // 16 * 16) for c in order]
    done[-1] = tok_dev

    def piece(ends, c):
        start = ends[c - 1] if c else 0
        return pl.ds(start, ends[c] - start)

    barrier = pltpu.get_barrier_semaphore()
    for m in range(1, tp):
        pl.semaphore_signal(barrier, inc=1, device_id=(me, flip(m)), device_id_type=MESH)
    for k in range(1, ep):
        pl.semaphore_signal(
            barrier, inc=1, device_id=(lax.rem(me + k, ep), t), device_id_type=MESH
        )
    pl.semaphore_wait(barrier, tp + ep - 2)

    def z_copy(c, k):
        rows_c = piece(need, c)
        return remote(
            tok.at[rows_c, :], near.at[k, rows_c, :], z_send.at[c, k], z_recv.at[c, k],
            lax.rem(me + k, ep), t,
        )

    for c in order:
        if piece(need, c).size:
            for k in range(1, ep):
                z_copy(c, k).start()

    def gain_copy(m):
        return remote(
            gain, gain_all.at[:, cols(0)], g_send.at[m], g_recv.at[m], me, flip(m)
        )

    def gain_wait(m):
        remote(gain, gain_all.at[:, cols(m)], g_send.at[m], g_recv.at[m], me, flip(m)).wait_recv()

    for m in range(1, tp):
        gain_copy(m).start()
    gain_all[:, cols(0)] = gain[...]

    chosen_row[...] = jnp.full(chosen_row.shape, -1.0, f32)
    aff_row[...] = jnp.zeros(aff_row.shape, f32)
    chosen_row[:, :count] = chosen[...].astype(f32)
    aff_row[:, :count] = aff[...]
    diagonal = lax.broadcasted_iota(jnp.int32, (rows, rows), 0) == lax.broadcasted_iota(
        jnp.int32, (rows, rows), 1
    )
    given = jnp.sum(jnp.where(diagonal, chosen_row[...], 0.0), axis=1, keepdims=True)
    factor = jnp.sum(jnp.where(diagonal, aff_row[...], 0.0), axis=1, keepdims=True)

    owners = [lax.rem(me + q, ep) for q in range(ep)]
    lane = lax.broadcasted_iota(jnp.int32, (rows, tok_dev), 1)
    sub = lax.broadcasted_iota(jnp.int32, (tok_dev, rows), 0)
    taken_row, taken_col = [], []
    for q in range(ep):
        match = given == (lane + owners[q] * tok_dev).astype(f32)
        taken_row.append(jnp.sum(match.astype(f32), axis=0, keepdims=True))
        aff_token[q] = jnp.sum(jnp.where(match, factor, 0.0), axis=0, keepdims=True)
        match = chosen_row[...] == (sub + owners[q] * tok_dev).astype(f32)
        taken_col.append(jnp.sum(match.astype(f32), axis=1, keepdims=True))
    down_index = lax.broadcasted_iota(jnp.int32, (tok_dev, tok_dev), 0) * ep
    across_index = lax.broadcasted_iota(jnp.int32, (tok_dev, tok_dev), 1) * ep
    for q in range(ep):
        ahead = jnp.zeros((tok_dev, tok_dev), f32)
        above = jnp.zeros((tok_dev, tok_dev), f32)
        for p in range(ep):
            ahead = ahead + jnp.where(
                down_index + owners[p] < across_index + owners[q], taken_col[p], 0.0
            )
            above = above + jnp.where(
                across_index + owners[p] < down_index + owners[q], taken_row[p], 0.0
            )
        slot_row[q] = jnp.where(taken_row[q] > 0, jnp.sum(ahead, axis=0, keepdims=True), -1.0)
        slot_col[q] = jnp.where(taken_col[q] > 0, jnp.sum(above, axis=1, keepdims=True), -1.0)

    def span(c):
        return pl.ds(c * size, size)

    routes = {
        1: (0, None, 1), 2: (0, None, 2), 4: (0, None, 4),
        3: (2, None, 1), 6: (2, 0, 4), 5: (4, None, 1), 8: (4, 1, 2),
        7: (6, 0, 1), 9: (6, 1, 1),
    }

    def ag_block(c, m, part_of):
        if part_of is None:
            return full.at[flip(m), span(c), :]
        return full.at[flip(m), pl.ds(c * size + part_of * half, half), :]

    def ag_copy(c, s):
        m, part_of, to = routes[s]
        block = ag_block(c, m, part_of)
        return remote(block, block, ag_send.at[c, s], ag_recv.at[c, s], me, flip(to))

    def ag_wait(c, s):
        m, part_of, to = routes[s]
        block = ag_block(c, m ^ to, part_of)
        remote(block, block, ag_send.at[c, s], ag_recv.at[c, s], me, flip(to)).wait_recv()

    def pick(c):
        if piece(need, c).size:
            for k in range(1, ep):
                z_copy(c, k).wait_recv()
        low, high = least[c], need[c]
        place = (lax.broadcasted_iota(jnp.int32, (size, high - low), 0) + c * size).astype(f32)
        total = jnp.zeros((size, width), f32)
        scale = jnp.zeros((size, high - low), f32)
        for k in range(ep):
            q = (ep - k) % ep
            hot = (place == slot_row[q, :, low:high]).astype(f32)
            scale = scale + hot * aff_token[q, :, low:high]
            block = tok[low:high, :] if k == 0 else near[k, low:high, :]
            total = total + jnp.dot(hot.astype(bf16), block, preferred_element_type=f32)
        aff_col[span(c), :] = jnp.sum(scale, axis=1, keepdims=True)
        full[t, span(c), :] = total.astype(bf16)
        for s in (2, 4, 1):
            ag_copy(c, s).start()

    def forward(c, stages):
        for s, onward in stages:
            ag_wait(c, s)
            for after in onward:
                ag_copy(c, after).start()

    first = ((2, (6, 3)), (4, (8, 5)))
    second = ((6, (7,)), (8, (9,)))

    sums = (
        (2, 0, 0, 2), (4, 1, 0, 4), (6, 0, 1, 2), (6, 1, 1, 4), (4, 0, 2, 4), (2, 1, 2, 2),
    )

    def r2_copy(c, s):
        m, part_of, slot, to = sums[s]
        rows_h = pl.ds(part_of * half, half)
        return remote(
            part.at[c, m, rows_h, :], got2.at[c, slot, rows_h, :],
            r2_send.at[c, s], r2_recv.at[c, s], me, flip(to),
        )

    def relay(c):
        for s, m, part_of in ((2, 4, 0), (3, 2, 1)):
            rows_h = pl.ds(part_of * half, half)
            r2_copy(c, s).wait_recv()
            part[c, m, rows_h, :] = (
                keep[c, part_of] + got2[c, 1, rows_h, :].astype(f32)
            ).astype(bf16)
            r2_copy(c, s + 2).start()

    def finish(c):
        for s in (0, 1, 4, 5):
            r2_copy(c, s).wait_recv()
        total = own[span(c), :] + got2[c, 0].astype(f32) + got2[c, 2].astype(f32)
        weighted[span(c), :] = (total * aff_col[span(c), :]).astype(bf16)
        if piece(done, c).size:
            for k in list(range(1, ep)) + [0]:
                at_tokens(c, k)

    def at_tokens(c, k):
        rows_c, slots = piece(done, c), size * (c + 1)
        place = lax.broadcasted_iota(jnp.int32, (rows_c.size, slots), 1).astype(f32)
        hot = (slot_col[k, rows_c, :] == place).astype(f32).astype(bf16)
        back[k, rows_c, :] = jnp.dot(
            hot, weighted[:slots, :], preferred_element_type=f32
        ).astype(bf16)
        if k:
            back_copy(c, k).start()

    def back_copy(c, k):
        rows_c = piece(done, c)
        return remote(
            back.at[k, rows_c, :], got_back.at[k, rows_c, :], b_send.at[c, k], b_recv.at[c, k],
            lax.rem(me + k, ep), t,
        )

    tile = min(ff, 256)
    pick(0)
    for c in order[1:]:
        pick(c)
        if c == 1:
            forward(0, first)
            forward(1, first)
            forward(0, second)
    for m in range(1, tp):
        gain_wait(m)
    for position, c in enumerate(order):
        for s in (1, 3, 5, 7, 9):
            ag_wait(c, s)
        square_sum = jnp.zeros((size, 1), f32)
        for b in range(tp):
            floats = full[b, span(c), :].astype(f32)
            square_sum = square_sum + jnp.sum(floats * floats, axis=1, keepdims=True)
        scale = lax.rsqrt(square_sum / d + EPS)
        for b in range(tp):
            at = slice(b * width, (b + 1) * width)
            floats = full[b, span(c), :].astype(f32)
            normed[:, at] = (floats * scale * gain_all[:, at]).astype(bf16)
        if position == 0:
            weights[0].wait()
            weights[1].wait()

        @pl.loop(0, ff // tile)
        def _(j):
            units = pl.ds(pl.multiple_of(j * tile, LANES), tile)
            gate = jnp.dot(normed[...], wg[:, units], preferred_element_type=f32)
            upward = jnp.dot(normed[...], wu[:, units], preferred_element_type=f32)
            hidden[:, units] = (gate / (1.0 + jnp.exp(-gate)) * upward).astype(bf16)

        if position + 1 < chunks:
            if position + 2 < chunks:
                forward(position + 2, first)
            forward(position + 1, second)
        if position:
            relay(position - 1)
        if position == 0:
            weights[2].wait()

        def down(m):
            return jnp.dot(hidden[...], wd[:, cols(m)], preferred_element_type=f32)

        for m in odds:
            part[c, m] = down(m).astype(bf16)
            remote(
                part.at[c, m], got1.at[c, m - 1], r1_send.at[c, m], r1_recv.at[c, m - 1],
                me, flip(1),
            ).start()
        for m in evens + [0]:
            mine = down(m)
            remote(
                part.at[c, m + 1], got1.at[c, m], r1_send.at[c, m + 1], r1_recv.at[c, m],
                me, flip(1),
            ).wait_recv()
            mine = mine + got1[c, m].astype(f32)
            if m == 6:
                part[c, 6] = mine.astype(bf16)
                r2_copy(c, 2).start()
                r2_copy(c, 3).start()
            elif m:
                part_of = 0 if m == 2 else 1
                sent, kept = pl.ds(part_of * half, half), (1 - part_of) * half
                part[c, m, sent, :] = mine[part_of * half : part_of * half + half].astype(bf16)
                r2_copy(c, part_of).start()
                keep[c, 1 - part_of] = mine[kept : kept + half]
            else:
                own[span(c), :] = mine

        if position >= LAG:
            finish(position - LAG)
    relay(chunks - 1)
    for c in order[max(0, chunks - LAG):]:
        finish(c)

    for c in order:
        if piece(done, c).size:
            rows_c = piece(done, c)
            mix = back[0, rows_c, :].astype(f32)
            for k in range(1, ep):
                back_copy(c, k).wait_recv()
                mix = mix + got_back[k, rows_c, :].astype(f32)
            out[rows_c, :] = mix.astype(bf16)

    for m in range(1, tp):
        gain_copy(m).wait_send()
    for c in order:
        for k in range(1, ep):
            if piece(need, c).size:
                z_copy(c, k).wait_send()
            if piece(done, c).size:
                back_copy(c, k).wait_send()
        for s in routes:
            ag_copy(c, s).wait_send()
        for s in range(len(sums)):
            r2_copy(c, s).wait_send()
        for m in odds:
            remote(
                part.at[c, m], got1.at[c, m - 1], r1_send.at[c, m], r1_recv.at[c, m - 1],
                me, flip(1),
            ).wait_send()


def fused(ep, tp, tokens, norm_gain, chosen, affinity, w_gate, w_up, w_down):
    tok_dev, width = tokens.shape
    d, ff = w_gate.shape[1:]
    count = chosen.shape[1]
    step = 32 * CHUNKS
    rows = -(-count // step) * step
    size = rows // CHUNKS
    f32, bf16 = jnp.float32, jnp.bfloat16
    vmem = pl.BlockSpec(memory_space=pltpu.VMEM)
    hbm = pl.BlockSpec(memory_space=pl.ANY)
    dma = pltpu.SemaphoreType.DMA
    return pl.pallas_call(
        functools.partial(kernel, ep, tp, CHUNKS),
        out_shape=jax.ShapeDtypeStruct((tok_dev, width), bf16),
        in_specs=[vmem] * 4 + [hbm] * 3,
        out_specs=vmem,
        scratch_shapes=[
            pltpu.VMEM((d, ff), bf16),
            pltpu.VMEM((d, ff), bf16),
            pltpu.VMEM((ff, d), bf16),
            pltpu.VMEM((tp, rows, width), bf16),
            pltpu.VMEM((size, d), bf16),
            pltpu.VMEM((size, ff), bf16),
            pltpu.VMEM((CHUNKS, tp, size, width), bf16),
            pltpu.VMEM((CHUNKS, tp, size, width), bf16),
            pltpu.VMEM((CHUNKS, tp, size, width), bf16),
            pltpu.VMEM((rows, width), f32),
            pltpu.VMEM((rows, width), bf16),
            pltpu.VMEM((ep, tok_dev, width), bf16),
            pltpu.VMEM((ep, tok_dev, width), bf16),
            pltpu.VMEM((ep, tok_dev, width), bf16),
            pltpu.VMEM((1, rows), f32),
            pltpu.VMEM((1, rows), f32),
            pltpu.VMEM((ep, 1, tok_dev), f32),
            pltpu.VMEM((ep, 1, tok_dev), f32),
            pltpu.VMEM((ep, tok_dev, 1), f32),
            pltpu.VMEM((rows, 1), f32),
            pltpu.VMEM((1, d), f32),
            pltpu.VMEM((CHUNKS, 2, size // 2, width), f32),
            dma((3,)),
            dma((tp,)),
            dma((tp,)),
            dma((CHUNKS, ep)),
            dma((CHUNKS, ep)),
            dma((CHUNKS, 2 * tp)),
            dma((CHUNKS, 2 * tp)),
            dma((CHUNKS, tp)),
            dma((CHUNKS, tp)),
            dma((CHUNKS, tp)),
            dma((CHUNKS, tp)),
            dma((CHUNKS, ep)),
            dma((CHUNKS, ep)),
        ],
        compiler_params=pltpu.CompilerParams(
            collective_id=0, has_side_effects=True, vmem_limit_bytes=VMEM_BYTES
        ),
    )(tokens, norm_gain[None, :], chosen, affinity, w_gate, w_up, w_down)


EPS = 1e-06


def plain(tokens, norm_gain, chosen, affinity, w_gate, w_up, w_down):
    tok_dev, width_part = tokens.shape
    ep_count = lax.axis_size("ep")
    floats = tokens.astype(jnp.float32)
    square_sum = lax.psum(jnp.sum(floats * floats, axis=1), "tp")
    normed = (floats * lax.rsqrt(square_sum / w_gate.shape[1] + EPS)[:, None] * norm_gain[None, :]).astype(
        jnp.bfloat16
    )
    own_choice = chosen[0]
    chosen_count = own_choice.shape[0]
    bound_rows = min(tok_dev, 2 * chosen_count // ep_count)
    slot_ids = jnp.arange(bound_rows, dtype=jnp.int32)
    positions = jnp.arange(chosen_count, dtype=jnp.int32)
    every_token = lax.all_gather(normed, "ep", axis=0, tiled=True)
    picked = every_token[own_choice]
    piece = lax.all_gather(picked, "tp", axis=1, tiled=True)
    gate_rows = w_gate[0]
    up_rows = w_up[0]
    gate = jnp.dot(piece, gate_rows, preferred_element_type=jnp.float32)
    upward = jnp.dot(piece, up_rows, preferred_element_type=jnp.float32)
    hidden = (jax.nn.silu(gate) * upward).astype(jnp.bfloat16)
    columns = w_down[0]
    summed = lax.psum_scatter(
        lax.dot_general(
            columns, hidden, (((0,), (1,)), ((), ())), preferred_element_type=jnp.float32
        ).astype(jnp.bfloat16),
        "tp",
        scatter_dimension=0,
        tiled=True,
    ).astype(jnp.float32)
    weighted = (summed * affinity[0][None, :]).astype(jnp.bfloat16).T
    owner = own_choice // tok_dev
    owner_local = own_choice - owner * tok_dev
    owner_hot = owner[:, None] == jnp.arange(ep_count, dtype=jnp.int32)[None, :]
    running = jnp.cumsum(owner_hot.astype(jnp.int32), axis=0)
    place = jnp.sum(jnp.where(owner_hot, running, 0), axis=1) - 1
    back_match = owner_hot.T[:, None, :] & (place[None, None, :] == slot_ids[None, :, None])
    back_filled = jnp.any(back_match, axis=2)
    back_pick = jnp.sum(jnp.where(back_match, positions[None, None, :], 0), axis=2)
    back_rows = jnp.where(back_filled[..., None], weighted[back_pick], jnp.zeros((), jnp.bfloat16))
    back_token = jnp.where(back_filled, owner_local[back_pick], tok_dev)
    got_back, got_token = (
        lax.all_to_all(back_rows, "ep", split_axis=0, concat_axis=0, tiled=True),
        lax.all_to_all(back_token, "ep", split_axis=0, concat_axis=0, tiled=True),
    )
    total = jnp.zeros((tok_dev, width_part), jnp.float32)
    total = total.at[got_token.reshape(-1)].add(
        got_back.reshape(-1, width_part).astype(jnp.float32), mode="drop"
    )
    return total.astype(jnp.bfloat16)


def solution(mesh):
    ep, tp = mesh.shape["ep"], mesh.shape["tp"]

    def local(tokens, *rest):
        whole_lanes = tokens.shape[1] % LANES == 0 and rest[3].shape[2] % LANES == 0
        if whole_lanes and tp == 2**3:
            return fused(ep, tp, tokens, *rest)
        return plain(tokens, *rest)

    in_specs = (
        P("ep", "tp"),
        P("tp"),
        P("ep", None),
        P("ep", None),
        P("ep", None, "tp"),
        P("ep", None, "tp"),
        P("ep", "tp", None),
    )
    out_specs = P("ep", "tp")
    return jax.shard_map(local, mesh=mesh, in_specs=in_specs, out_specs=out_specs, check_vma=False)
```

profile of v0, /device:TPU:0, one launch (start us, length us, event | category | flops | bytes accessed | tf_op | source)
XLA Modules:
  0.0 53.7 jit_solution(13035145761612852349)
XLA Ops:
  0.0 52.2 %shard_map.73 = bf16[168,256]{1,0:T(8,128)(2,1)} custom-call(bf16[168,256]{1,0:T(8,128)(2,1)} %tok.1, f32[1,256]{1,0:T(1,128)} %bitcast.1, s32[1,504]{1,0:T(1,128)} %chosen.1, f32[1,504]{1,0:T(1,128)} %aff.1, bf16[1,2048,1024]{2,1,0:T(8,128)(2,1)} %wg_hbm.1, bf16[1,2048,1024]{2,1,0:T(8,128)(2,1)} %wu_hbm.1, bf16[1,1024,2048]{2,1,0:T(8,128)(2,1)} %wd_hbm.1), custom_call_target="tpu_custom_call" | custom-call | tf_op jit(solution)/shard_map/pallas_call | solution.py:358
  52.2 1.5 %copy.9 = bf16[168,256]{1,0:T(8,128)(2,1)} copy(bf16[168,256]{1,0:T(8,128)(2,1)} %shard_map.73) | data formatting | bytes 172032
where the time goes:
time: 53.9 us; the launch traced here: 53.7 us
  Pallas kernels  52.2 us (97%)
  local copies, waits for them, and re-layouts  1.53 us (3%)
    pallas_call x1, Pallas kernels, fused(): pl.pallas_call(functools.partial(kernel, ep, tp, CHUNKS), out_shape=jax.S...  52.2 us
    unnamed x1, local copies, waits for them, and re-layouts  1.53 us

commit v1 on v0

v1 whole, which is shorter than its diff:
```python
import functools

import jax
import jax.numpy as jnp
from jax import lax
from jax.experimental import pallas as pl
from jax.experimental.pallas import tpu as pltpu
from jax.sharding import PartitionSpec as P

MESH = pl.DeviceIdType.MESH
VMEM_BYTES = 67_043_328
LANES = 128
SHARES = (1, 1, 1, 1)
AG_ACROSS = (0, 1, 2, 3)
SUM_ACROSS = (0, 1, 2, 3)


def kernel(
    ep, tp, sizes,
    tok_hbm, gain_hbm, chosen_hbm, aff_hbm, wg_hbm, wu_hbm, wd_hbm,
    out,
    tok, gain, chosen, aff, wg, wu, wd, full, hidden, part, got1, got2, sums_even, own, weighted,
    near, back, got_back, chosen_row, aff_row, slot_row, slot_col,
    aff_col, square_row, keep, in_sem, w_sem, s_send, s_recv, z_send, z_recv, ag_send, ag_recv,
    r1_send, r1_recv, r2_send, r2_recv, b_send, b_recv,
):
    me = lax.axis_index("ep")
    t = lax.axis_index("tp")
    tok_dev, width = tok.shape
    rows = full.shape[1]
    d = wg.shape[0]
    count = chosen.shape[1]
    ff = wg.shape[1]
    chunks = len(sizes)
    starts = [sum(sizes[:c]) for c in range(chunks)]
    ends = [sum(sizes[: c + 1]) for c in range(chunks)]
    f32, bf16 = jnp.float32, jnp.bfloat16
    scope = jax.named_scope

    def flip(m):
        index, bit = t, 1
        while bit <= m:
            if m & bit:
                index = index + bit - 2 * bit * ((t // bit) % 2)
            bit *= 2
        return index

    def cols(m):
        return pl.ds(pl.multiple_of(flip(m) * width, LANES), width)

    def remote(src, dst, send, recv, ep_to, tp_to):
        return pltpu.make_async_remote_copy(
            src_ref=src, dst_ref=dst, send_sem=send, recv_sem=recv,
            device_id=(ep_to, tp_to), device_id_type=MESH,
        )

    def whole(ref, send, recv):
        return remote(ref, ref, send, recv, me, flip(1))

    evens = [6, 2, 4, 0]
    order = list(range(chunks))
    weights = [
        pltpu.make_async_copy(h.at[0], v, w_sem.at[i])
        for i, (h, v) in enumerate(((wg_hbm, wg), (wu_hbm, wu), (wd_hbm, wd)))
    ]
    inputs = [
        pltpu.make_async_copy(h, v, in_sem.at[i])
        for i, (h, v) in enumerate(
            ((tok_hbm, tok), (gain_hbm, gain), (chosen_hbm, chosen), (aff_hbm, aff))
        )
    ]
    for copy in inputs:
        copy.start()

    spare = ep * tok_dev - count
    need = [min(tok_dev, -(-(-(-(ends[c] + spare) // ep)) // 16) * 16) for c in order]
    need[-1] = tok_dev
    least = [starts[c] // ep // 16 * 16 for c in order]
    done = [min(tok_dev, ends[c] // ep // 16 * 16) for c in order]
    done[-1] = tok_dev

    def piece(stops, c):
        start = stops[c - 1] if c else 0
        return pl.ds(start, stops[c] - start)

    barrier = pltpu.get_barrier_semaphore()
    for m in range(1, tp):
        pl.semaphore_signal(barrier, inc=1, device_id=(me, flip(m)), device_id_type=MESH)
    for k in range(1, ep):
        pl.semaphore_signal(
            barrier, inc=1, device_id=(lax.rem(me + k, ep), t), device_id_type=MESH
        )
    with scope("inputs"):
        for copy in inputs:
            copy.wait()
    for copy in weights:
        copy.start()
    with scope("barrier"):
        pl.semaphore_wait(barrier, tp + ep - 2)

    def z_copy(c, k):
        rows_c = piece(need, c)
        return remote(
            tok.at[rows_c, :], near.at[k, rows_c, :], z_send.at[0], z_recv.at[c],
            lax.rem(me + k, ep), t,
        )

    def z_start(c):
        if piece(need, c).size:
            for k in range(1, ep):
                z_copy(c, k).start()

    z_start(0)

    with scope("index"):
        chosen_row[...] = jnp.full(chosen_row.shape, -1.0, f32)
        aff_row[...] = jnp.zeros(aff_row.shape, f32)
        chosen_row[:, :count] = chosen[...].astype(f32)
        aff_row[:, :count] = aff[...]
        diagonal = lax.broadcasted_iota(jnp.int32, (rows, rows), 0) == lax.broadcasted_iota(
            jnp.int32, (rows, rows), 1
        )
        given = jnp.sum(jnp.where(diagonal, chosen_row[...], 0.0), axis=1, keepdims=True)
        factor = jnp.sum(jnp.where(diagonal, aff_row[...], 0.0), axis=1, keepdims=True)

        owners = [lax.rem(me + q, ep) for q in range(ep)]
        lane = lax.broadcasted_iota(jnp.int32, (rows, tok_dev), 1)
        sub = lax.broadcasted_iota(jnp.int32, (tok_dev, rows), 0)
        taken_row, taken_col, aff_token = [], [], []
        for q in range(ep):
            match = given == (lane + owners[q] * tok_dev).astype(f32)
            taken_row.append(jnp.sum(match.astype(f32), axis=0, keepdims=True))
            aff_token.append(jnp.sum(jnp.where(match, factor, 0.0), axis=0, keepdims=True))
            match = chosen_row[...] == (sub + owners[q] * tok_dev).astype(f32)
            taken_col.append(jnp.sum(match.astype(f32), axis=1, keepdims=True))
        down_index = lax.broadcasted_iota(jnp.int32, (tok_dev, tok_dev), 0) * ep
        across_index = lax.broadcasted_iota(jnp.int32, (tok_dev, tok_dev), 1) * ep
        place_all = lax.broadcasted_iota(jnp.int32, (rows, tok_dev), 0).astype(f32)
        factor_sum = jnp.zeros((rows, tok_dev), f32)
        for q in range(ep):
            ahead = jnp.zeros((tok_dev, tok_dev), f32)
            above = jnp.zeros((tok_dev, tok_dev), f32)
            for p in range(ep):
                ahead = ahead + jnp.where(
                    down_index + owners[p] < across_index + owners[q], taken_col[p], 0.0
                )
                above = above + jnp.where(
                    across_index + owners[p] < down_index + owners[q], taken_row[p], 0.0
                )
            slot_row[q] = jnp.where(
                taken_row[q] > 0, jnp.sum(ahead, axis=0, keepdims=True), -1.0
            )
            slot_col[q] = jnp.where(
                taken_col[q] > 0, jnp.sum(above, axis=1, keepdims=True), -1.0
            )
            factor_sum = factor_sum + jnp.where(place_all == slot_row[q], aff_token[q], 0.0)
        aff_col[...] = jnp.sum(factor_sum, axis=1, keepdims=True)

    def span(c):
        return pl.ds(starts[c], sizes[c])

    def part_rows(c, part_of):
        half = sizes[c] // 2
        return pl.ds(starts[c] + part_of * half, half)

    routes = {
        1: (0, None, 1), 2: (0, None, 2), 4: (0, None, 4),
        3: (2, None, 1), 6: (2, 0, 4), 5: (4, None, 1), 8: (4, 1, 2),
        7: (6, 0, 1), 9: (6, 1, 1),
    }

    across = {
        1: (0, None, 1), 2: (0, None, 2), 4: (0, None, 4), 6: (0, None, 6),
        3: (2, None, 1), 5: (4, None, 1), 7: (6, None, 1),
    }
    ag_slot = {2: 1, 4: 2, 6: 3, 8: 4, 1: 0, 3: 0, 5: 0, 7: 0, 9: 0}

    def route(c, s):
        return (across if c in AG_ACROSS else routes)[s]

    def ag_block(c, m, part_of):
        return full.at[flip(m), span(c) if part_of is None else part_rows(c, part_of), :]

    def ag_copy(c, s):
        m, part_of, to = route(c, s)
        block = ag_block(c, m, part_of)
        return remote(block, block, ag_send.at[0], ag_recv.at[c, ag_slot[s]], me, flip(to))

    def ag_wait(c, s):
        m, part_of, to = route(c, s)
        block = ag_block(c, m ^ to, part_of)
        whole(block, ag_send.at[0], ag_recv.at[c, ag_slot[s]]).wait_recv()

    def square_copy(c, m):
        return remote(
            square_row.at[c, 0], square_row.at[c, m], s_send.at[0], s_recv.at[c], me, flip(m)
        )

    def pick(c):
        low, high, size = least[c], need[c], sizes[c]
        place = (
            lax.broadcasted_iota(jnp.int32, (size, high - low), 0) + starts[c]
        ).astype(f32)
        hots = []
        for k in range(ep):
            q = (ep - k) % ep
            hots.append((place == slot_row[q, :, low:high]).astype(f32).astype(bf16))
        with scope(f"zwait{c}"):
            if piece(need, c).size:
                rows_c = piece(need, c)
                whole(near.at[1:, rows_c, :], z_send.at[0], z_recv.at[c]).wait_recv()
        with scope(f"pick{c}"):
            total = jnp.zeros((size, width), f32)
            for k in range(ep):
                block = tok[low:high, :] if k == 0 else near[k, low:high, :]
                total = total + jnp.dot(hots[k], block, preferred_element_type=f32)
            full[t, span(c), :] = (total * gain[...]).astype(bf16)
            for s in (6, 2, 4, 1) if c in AG_ACROSS else (2, 4, 1):
                ag_copy(c, s).start()
            diagonal = lax.broadcasted_iota(jnp.int32, (size, size), 0) == (
                lax.broadcasted_iota(jnp.int32, (size, size), 1)
            )
            squares = jnp.sum(total * total, axis=1, keepdims=True)
            square_row[c, 0, :, :size] = jnp.sum(
                jnp.where(diagonal, squares, 0.0), axis=0, keepdims=True
            )
            for m in range(1, tp):
                square_copy(c, m).start()

    def forward(c, stages):
        with scope(f"fwd{c}_{stages[0][0]}"):
            for s, onward in stages:
                ag_wait(c, s)
                for after in onward:
                    ag_copy(c, after).start()

    first = ((2, (6, 3)), (4, (8, 5)))
    second = ((6, (7,)), (8, (9,)))

    sums = (
        (2, 0, 0, 2), (4, 1, 0, 4), (6, 0, 1, 2), (6, 1, 1, 4), (4, 0, 2, 4), (2, 1, 2, 2),
    )

    def r1_copy(c, i):
        return remote(
            part.at[2 * i + 1, span(c), :], got1.at[i, span(c), :],
            r1_send.at[0], r1_recv.at[c, int(i == 3)], me, flip(1),
        )

    def r2_copy(c, s):
        m, part_of, slot, to = sums[s]
        rows_h = part_rows(c, part_of)
        return remote(
            part.at[m, rows_h, :], got2.at[slot, rows_h, :],
            r2_send.at[0], r2_recv.at[c, {2: 1, 3: 2}.get(s, 0)], me, flip(to),
        )

    tile = min(ff, 256)

    def gate_up(c):
        with scope(f"agwait{c}"):
            whole(full.at[: tp // 2, span(c), :], ag_send.at[0], ag_recv.at[c, 0]).wait_recv()
            whole(square_row.at[c, 1:], s_send.at[0], s_recv.at[c]).wait_recv()
        with scope(f"gateup{c}"):
            size = sizes[c]
            diagonal = lax.broadcasted_iota(jnp.int32, (size, size), 0) == (
                lax.broadcasted_iota(jnp.int32, (size, size), 1)
            )
            squares = square_row[c, 0, :, :size]
            for m in range(1, tp):
                squares = squares + square_row[c, m, :, :size]
            squares = jnp.sum(jnp.where(diagonal, squares, 0.0), axis=1, keepdims=True)
            scale = lax.rsqrt(squares / d + EPS)
            for j in range(ff // tile):
                units = slice(j * tile, (j + 1) * tile)
                gate = jnp.zeros((sizes[c], tile), f32)
                upward = jnp.zeros((sizes[c], tile), f32)
                for b in range(tp):
                    at = slice(b * width, (b + 1) * width)
                    gate = gate + jnp.dot(
                        full[b, span(c), :], wg[at, units], preferred_element_type=f32
                    )
                    upward = upward + jnp.dot(
                        full[b, span(c), :], wu[at, units], preferred_element_type=f32
                    )
                gate, upward = gate * scale, upward * scale
                hidden[c % 2, : sizes[c], units] = (
                    gate / (1.0 + jnp.exp(-gate)) * upward
                ).astype(bf16)

    def down(c):
        def block(m):
            return jnp.dot(
                hidden[c % 2, : sizes[c], :], wd[:, cols(m)], preferred_element_type=f32
            )

        with scope(f"odd{c}"):
            for m in evens:
                part[m + 1, span(c), :] = block(m + 1).astype(bf16)
            if c == chunks - 1:
                for m in evens:
                    r1_copy(c, m // 2).start()
        with scope(f"even{c}"):
            for m in evens:
                sums_even[m // 2, span(c), :] = block(m)
            if c < chunks - 1:
                for m in evens:
                    r1_copy(c, m // 2).start()

    def sum_copy(c, m):
        return remote(
            part.at[m, span(c), :], got2.at[m // 2 - 1, span(c), :],
            r2_send.at[0], r2_recv.at[c, 0], me, flip(m),
        )

    def reduce(c):
        half = sizes[c] // 2
        with scope(f"reduce{c}"):
            for m in evens:
                if m == 6:
                    whole(got1.at[3, span(c), :], r1_send.at[0], r1_recv.at[c, 1]).wait_recv()
                elif m == 2:
                    whole(got1.at[:3, span(c), :], r1_send.at[0], r1_recv.at[c, 0]).wait_recv()
                mine = sums_even[m // 2, span(c), :] + got1[m // 2, span(c), :].astype(f32)
                if m and c in SUM_ACROSS:
                    part[m, span(c), :] = mine.astype(bf16)
                    sum_copy(c, m).start()
                elif m == 6:
                    part[6, span(c), :] = mine.astype(bf16)
                    r2_copy(c, 2).start()
                    r2_copy(c, 3).start()
                elif m:
                    part_of = 0 if m == 2 else 1
                    sent, kept = part_of * half, (1 - part_of) * half
                    part[m, part_rows(c, part_of), :] = mine[sent : sent + half].astype(bf16)
                    r2_copy(c, part_of).start()
                    keep[part_rows(c, 1 - part_of), :] = mine[kept : kept + half]
                else:
                    own[span(c), :] = mine

    def relay(c):
        if c in SUM_ACROSS:
            return
        with scope(f"relay{c}"):
            for s, m, part_of in ((2, 4, 0), (3, 2, 1)):
                rows_h = part_rows(c, part_of)
                r2_copy(c, s).wait_recv()
                part[m, rows_h, :] = (
                    keep[rows_h, :] + got2[1, rows_h, :].astype(f32)
                ).astype(bf16)
                r2_copy(c, s + 2).start()

    def finish(c):
        rows_c = piece(done, c)
        low = max(0, (starts[c] - spare) // LANES * LANES)
        hots = []
        if rows_c.size:
            place = lax.broadcasted_iota(jnp.int32, (rows_c.size, ends[c] - low), 1) + low
            for k in range(ep):
                hots.append(
                    (slot_col[k, rows_c, :] == place.astype(f32)).astype(f32).astype(bf16)
                )
        with scope(f"sumwait{c}"):
            whole(got2.at[: 3 if c in SUM_ACROSS else 2, span(c), :], r2_send.at[0], r2_recv.at[c, 0]).wait_recv()
        with scope(f"finish{c}"):
            at = span(c)
            total = own[at, :] + got2[0, at, :].astype(f32) + got2[2, at, :].astype(f32)
            if c in SUM_ACROSS:
                total = total + got2[1, at, :].astype(f32)
            weighted[at, :] = (total * aff_col[at, :]).astype(bf16)
            if rows_c.size:
                for k in range(ep):
                    back[k, rows_c, :] = jnp.dot(
                        hots[k], weighted[low : ends[c], :], preferred_element_type=f32
                    ).astype(bf16)
                for k in range(1, ep):
                    back_copy(c, k).start()

    def back_copy(c, k):
        rows_c = piece(done, c)
        return remote(
            back.at[k, rows_c, :], got_back.at[k, rows_c, :], b_send.at[0], b_recv.at[c],
            lax.rem(me + k, ep), t,
        )

    def mix(c):
        if piece(done, c).size:
            with scope(f"mix{c}"):
                rows_c = piece(done, c)
                total = back[0, rows_c, :].astype(f32)
                whole(got_back.at[1:, rows_c, :], b_send.at[0], b_recv.at[c]).wait_recv()
                for k in range(1, ep):
                    total = total + got_back[k, rows_c, :].astype(f32)
                out[rows_c, :] = total.astype(bf16)

    def fwd_a(c):
        forward(c, ((2, (3,)), (4, (5,))) if c in AG_ACROSS else first)

    def fwd_b(c):
        forward(c, ((6, (7,)),) if c in AG_ACROSS else second)

    def wait_weights(c):
        with scope("wwait"):
            weights[c].wait()

    steps = {
        "pick": pick, "A": fwd_a, "B": fwd_b, "gu": gate_up, "dn": down, "red": reduce,
        "rel": relay, "fin": finish, "mix": mix, "w": wait_weights, "z": z_start,
    }
    for name, c in ORDER:
        steps[name](c)

    with scope("tail"):
        for ref, send, recv in (
            (square_row.at[:, 1:], s_send, s_recv),
            (near.at[1:], z_send, s_recv),
            (got_back.at[1:], b_send, s_recv),
            (full.at[: tp - 1], ag_send, s_recv),
            (got2, r2_send, s_recv),
            (got1, r1_send, s_recv),
        ):
            whole(ref, send.at[0], recv.at[0]).wait_send()


ORDER = (
    ("z", 1), ("z", 2), ("z", 3), ("pick", 0), ("pick", 1), ("A", 0), ("B", 0), ("pick", 2),
    ("pick", 3), ("w", 0), ("w", 1), ("gu", 0), ("A", 1), ("B", 1), ("w", 2), ("dn", 0), ("A", 2),
    ("B", 2), ("gu", 1), ("red", 0), ("A", 3), ("B", 3), ("dn", 1), ("gu", 2), ("red", 1),
    ("rel", 0), ("dn", 2), ("gu", 3), ("red", 2), ("rel", 1), ("dn", 3), ("fin", 0), ("red", 3),
    ("rel", 2), ("fin", 1), ("rel", 3), ("fin", 2), ("fin", 3), ("mix", 0), ("mix", 1), ("mix", 2),
    ("mix", 3),
)


def fused(ep, tp, tokens, norm_gain, chosen, affinity, w_gate, w_up, w_down):
    tok_dev, width = tokens.shape
    d, ff = w_gate.shape[1:]
    count = chosen.shape[1]
    step = 32 * sum(SHARES)
    rows = -(-count // step) * step
    sizes = tuple(rows // sum(SHARES) * share for share in SHARES)
    largest = max(sizes)
    f32, bf16 = jnp.float32, jnp.bfloat16
    vmem = pl.BlockSpec(memory_space=pltpu.VMEM)
    hbm = pl.BlockSpec(memory_space=pl.ANY)
    dma = pltpu.SemaphoreType.DMA
    return pl.pallas_call(
        functools.partial(kernel, ep, tp, sizes),
        out_shape=pltpu.VMEM((tok_dev, width), bf16),
        in_specs=[hbm] * 7,
        out_specs=vmem,
        scratch_shapes=[
            pltpu.VMEM((tok_dev, width), bf16),
            pltpu.VMEM((1, width), f32),
            pltpu.VMEM((1, count), jnp.int32),
            pltpu.VMEM((1, count), f32),
            pltpu.VMEM((d, ff), bf16),
            pltpu.VMEM((d, ff), bf16),
            pltpu.VMEM((ff, d), bf16),
            pltpu.VMEM((tp, rows, width), bf16),
            pltpu.VMEM((2, largest, ff), bf16),
            pltpu.VMEM((tp, rows, width), bf16),
            pltpu.VMEM((tp // 2, rows, width), bf16),
            pltpu.VMEM((3, rows, width), bf16),
            pltpu.VMEM((tp // 2, rows, width), f32),
            pltpu.VMEM((rows, width), f32),
            pltpu.VMEM((rows, width), bf16),
            pltpu.VMEM((ep, tok_dev, width), bf16),
            pltpu.VMEM((ep, tok_dev, width), bf16),
            pltpu.VMEM((ep, tok_dev, width), bf16),
            pltpu.VMEM((1, rows), f32),
            pltpu.VMEM((1, rows), f32),
            pltpu.VMEM((ep, 1, tok_dev), f32),
            pltpu.VMEM((ep, tok_dev, 1), f32),
            pltpu.VMEM((rows, 1), f32),
            pltpu.VMEM((len(SHARES), tp, 1, -(-largest // LANES) * LANES), f32),
            pltpu.VMEM((rows, width), f32),
            dma((4,)),
            dma((3,)),
            dma((1,)),
            dma((len(SHARES),)),
            dma((1,)),
            dma((len(SHARES),)),
            dma((1,)),
            dma((len(SHARES), 5)),
            dma((1,)),
            dma((len(SHARES), 2)),
            dma((1,)),
            dma((len(SHARES), 3)),
            dma((1,)),
            dma((len(SHARES),)),
        ],
        compiler_params=pltpu.CompilerParams(
            collective_id=0, has_side_effects=True, vmem_limit_bytes=VMEM_BYTES - 2**20
        ),
    )(tokens, norm_gain[None, :], chosen, affinity, w_gate, w_up, w_down)


EPS = 1e-06


def plain(tokens, norm_gain, chosen, affinity, w_gate, w_up, w_down):
    tok_dev, width_part = tokens.shape
    ep_count = lax.axis_size("ep")
    floats = tokens.astype(jnp.float32)
    square_sum = lax.psum(jnp.sum(floats * floats, axis=1), "tp")
    normed = (floats * lax.rsqrt(square_sum / w_gate.shape[1] + EPS)[:, None] * norm_gain[None, :]).astype(
        jnp.bfloat16
    )
    own_choice = chosen[0]
    chosen_count = own_choice.shape[0]
    bound_rows = min(tok_dev, 2 * chosen_count // ep_count)
    slot_ids = jnp.arange(bound_rows, dtype=jnp.int32)
    positions = jnp.arange(chosen_count, dtype=jnp.int32)
    every_token = lax.all_gather(normed, "ep", axis=0, tiled=True)
    picked = every_token[own_choice]
    piece = lax.all_gather(picked, "tp", axis=1, tiled=True)
    gate_rows = w_gate[0]
    up_rows = w_up[0]
    gate = jnp.dot(piece, gate_rows, preferred_element_type=jnp.float32)
    upward = jnp.dot(piece, up_rows, preferred_element_type=jnp.float32)
    hidden = (jax.nn.silu(gate) * upward).astype(jnp.bfloat16)
    columns = w_down[0]
    summed = lax.psum_scatter(
        lax.dot_general(
            columns, hidden, (((0,), (1,)), ((), ())), preferred_element_type=jnp.float32
        ).astype(jnp.bfloat16),
        "tp",
        scatter_dimension=0,
        tiled=True,
    ).astype(jnp.float32)
    weighted = (summed * affinity[0][None, :]).astype(jnp.bfloat16).T
    owner = own_choice // tok_dev
    owner_local = own_choice - owner * tok_dev
    owner_hot = owner[:, None] == jnp.arange(ep_count, dtype=jnp.int32)[None, :]
    running = jnp.cumsum(owner_hot.astype(jnp.int32), axis=0)
    place = jnp.sum(jnp.where(owner_hot, running, 0), axis=1) - 1
    back_match = owner_hot.T[:, None, :] & (place[None, None, :] == slot_ids[None, :, None])
    back_filled = jnp.any(back_match, axis=2)
    back_pick = jnp.sum(jnp.where(back_match, positions[None, None, :], 0), axis=2)
    back_rows = jnp.where(back_filled[..., None], weighted[back_pick], jnp.zeros((), jnp.bfloat16))
    back_token = jnp.where(back_filled, owner_local[back_pick], tok_dev)
    got_back, got_token = (
        lax.all_to_all(back_rows, "ep", split_axis=0, concat_axis=0, tiled=True),
        lax.all_to_all(back_token, "ep", split_axis=0, concat_axis=0, tiled=True),
    )
    total = jnp.zeros((tok_dev, width_part), jnp.float32)
    total = total.at[got_token.reshape(-1)].add(
        got_back.reshape(-1, width_part).astype(jnp.float32), mode="drop"
    )
    return total.astype(jnp.bfloat16)


def solution(mesh):
    ep, tp = mesh.shape["ep"], mesh.shape["tp"]

    def local(tokens, *rest):
        whole_lanes = tokens.shape[1] % LANES == 0 and rest[3].shape[2] % LANES == 0
        if whole_lanes and tp == 2**3:
            return fused(ep, tp, tokens, *rest)
        return plain(tokens, *rest)

    in_specs = (
        P("ep", "tp"),
        P("tp"),
        P("ep", None),
        P("ep", None),
        P("ep", None, "tp"),
        P("ep", None, "tp"),
        P("ep", "tp", None),
    )
    out_specs = P("ep", "tp")
    return jax.shard_map(local, mesh=mesh, in_specs=in_specs, out_specs=out_specs, check_vma=False)
```

time: 53.9 us -> 43.2 us (0.80)
  Pallas kernels: 52.2 us -> 42.4 us
  local copies, waits for them, and re-layouts: 1.53 us -> 0.64 us
    pallas_call x1, Pallas kernels: 52.2 us -> 42.4 us  [fused(): pl.pallas_call(functools.partial(kernel, ep, tp, sizes), out_shape=pltpu....]
    unnamed x1, local copies, waits for them, and re-layouts: 1.53 us -> 0.64 us
where the time goes in v1:
time: 43.2 us; the launch traced here: 43.1 us
  Pallas kernels  42.4 us (98%)
  local copies, waits for them, and re-layouts  0.64 us (1%)
    pallas_call x1, Pallas kernels, fused(): pl.pallas_call(functools.partial(kernel, ep, tp, sizes), out_shape=pltpu....  42.4 us

profile of v1, /device:TPU:0, one launch (start us, length us, event | category | flops | bytes accessed | tf_op | source)
XLA Modules:
  0.0 43.1 jit_solution(1364482994425872126)
XLA Ops:
  0.0 42.4 %shard_map.73 = bf16[168,256]{1,0:T(8,128)(2,1)S(1)} custom-call(bf16[168,256]{1,0:T(8,128)(2,1)} %tok_hbm.1, f32[1,256]{1,0:T(1,128)} %bitcast.1, s32[1,504]{1,0:T(1,128)} %chosen_hbm.1, f32[1,504]{1,0:T(1,128)} %aff_hbm.1, bf16[1,2048,1024]{2,1,0:T(8,128)(2,1)} %wg_hbm.1, bf16[1,2048,1024]{2,1,0:T(8,128)(2,1)} %wu_hbm.1, bf16[1,1024,2048]{2,1,0:T(8,128)(2,1)} %wd_hbm.1), custom_call_target="tpu_custom_call" | custom-call | tf_op jit(solution)/shard_map/pallas_call | solution.py:447
  42.5 0.6 %copy.9 = bf16[168,256]{1,0:T(8,128)(2,1)} copy(bf16[168,256]{1,0:T(8,128)(2,1)S(1)} %shard_map.73) | data formatting | bytes 172032

commit v2 on v1

--- a/solution.py
+++ b/solution.py
@@ -105,9 +105,27 @@
             lax.rem(me + k, ep), t,
         )
 
+    def farthest_first():
+        after, before = ep - 1 - me, me
+        longer = (after - before + ep) // ep
+        gap = (2 * longer - 1) * (after - before)
+        short = (ep - 1 - gap) // 2
+        steps = []
+        for i in range(ep - 1):
+            alone = (gap - 1 - i + ep) // ep
+            far = longer * (ep - 1 - i) + (1 - longer) * i
+            pair = i - gap
+            near_by = me + (1 - 2 * ((pair + 2 * ep) % 2)) * (short - (pair + 2 * ep) // 2 + ep)
+            to = alone * far + (1 - alone) * near_by
+            steps.append(lax.rem(to - me + ep, ep))
+        return steps
+
+    hops = farthest_first()
+    hops = hops[:1] + hops[:0:-1]
+
     def z_start(c):
         if piece(need, c).size:
-            for k in range(1, ep):
+            for k in hops:
                 z_copy(c, k).start()
 
     z_start(0)
@@ -257,11 +275,26 @@
 
     tile = min(ff, 256)
 
+    scales = {}
+
     def gate_up(c):
+        gate_up_first(c)
+        gate_up_rest(c)
+
+    def gate_up_first(c):
+        gathered(c)
+        with scope(f"gateup{c}"):
+            gate_up_tiles(c, range(ff // tile // 2))
+
+    def gate_up_rest(c):
+        with scope(f"gaterest{c}"):
+            gate_up_tiles(c, range(ff // tile // 2, ff // tile))
+
+    def gathered(c):
         with scope(f"agwait{c}"):
             whole(full.at[: tp // 2, span(c), :], ag_send.at[0], ag_recv.at[c, 0]).wait_recv()
             whole(square_row.at[c, 1:], s_send.at[0], s_recv.at[c]).wait_recv()
-        with scope(f"gateup{c}"):
+        with scope(f"scale{c}"):
             size = sizes[c]
             diagonal = lax.broadcasted_iota(jnp.int32, (size, size), 0) == (
                 lax.broadcasted_iota(jnp.int32, (size, size), 1)
@@ -270,23 +303,25 @@
             for m in range(1, tp):
                 squares = squares + square_row[c, m, :, :size]
             squares = jnp.sum(jnp.where(diagonal, squares, 0.0), axis=1, keepdims=True)
-            scale = lax.rsqrt(squares / d + EPS)
-            for j in range(ff // tile):
-                units = slice(j * tile, (j + 1) * tile)
-                gate = jnp.zeros((sizes[c], tile), f32)
-                upward = jnp.zeros((sizes[c], tile), f32)
-                for b in range(tp):
-                    at = slice(b * width, (b + 1) * width)
-                    gate = gate + jnp.dot(
-                        full[b, span(c), :], wg[at, units], preferred_element_type=f32
-                    )
-                    upward = upward + jnp.dot(
-                        full[b, span(c), :], wu[at, units], preferred_element_type=f32
-                    )
-                gate, upward = gate * scale, upward * scale
-                hidden[c % 2, : sizes[c], units] = (
-                    gate / (1.0 + jnp.exp(-gate)) * upward
-                ).astype(bf16)
+            scales[c] = lax.rsqrt(squares / d + EPS)
+
+    def gate_up_tiles(c, tiles):
+        for j in tiles:
+            units = slice(j * tile, (j + 1) * tile)
+            gate = jnp.zeros((sizes[c], tile), f32)
+            upward = jnp.zeros((sizes[c], tile), f32)
+            for b in range(tp):
+                at = slice(b * width, (b + 1) * width)
+                gate = gate + jnp.dot(
+                    full[b, span(c), :], wg[at, units], preferred_element_type=f32
+                )
+                upward = upward + jnp.dot(
+                    full[b, span(c), :], wu[at, units], preferred_element_type=f32
+                )
+            gate, upward = gate * scales[c], upward * scales[c]
+            hidden[c % 2, : sizes[c], units] = (
+                gate / (1.0 + jnp.exp(-gate)) * upward
+            ).astype(bf16)
 
     def down(c):
         def block(m):
@@ -373,7 +408,7 @@
                     back[k, rows_c, :] = jnp.dot(
                         hots[k], weighted[low : ends[c], :], preferred_element_type=f32
                     ).astype(bf16)
-                for k in range(1, ep):
+                for k in hops:
                     back_copy(c, k).start()
 
     def back_copy(c, k):
@@ -404,7 +439,7 @@
             weights[c].wait()
 
     steps = {
-        "pick": pick, "A": fwd_a, "B": fwd_b, "gu": gate_up, "dn": down, "red": reduce,
+        "pick": pick, "A": fwd_a, "B": fwd_b, "gu": gate_up, "ga": gate_up_first, "gb": gate_up_rest, "dn": down, "red": reduce,
         "rel": relay, "fin": finish, "mix": mix, "w": wait_weights, "z": z_start,
     }
     for name, c in ORDER:
@@ -423,12 +458,12 @@
 
 
 ORDER = (
-    ("z", 1), ("z", 2), ("z", 3), ("pick", 0), ("pick", 1), ("A", 0), ("B", 0), ("pick", 2),
-    ("pick", 3), ("w", 0), ("w", 1), ("gu", 0), ("A", 1), ("B", 1), ("w", 2), ("dn", 0), ("A", 2),
-    ("B", 2), ("gu", 1), ("red", 0), ("A", 3), ("B", 3), ("dn", 1), ("gu", 2), ("red", 1),
-    ("rel", 0), ("dn", 2), ("gu", 3), ("red", 2), ("rel", 1), ("dn", 3), ("fin", 0), ("red", 3),
-    ("rel", 2), ("fin", 1), ("rel", 3), ("fin", 2), ("fin", 3), ("mix", 0), ("mix", 1), ("mix", 2),
-    ("mix", 3),
+    ("z", 1), ("pick", 0), ("z", 2), ("pick", 1), ("z", 3), ("A", 0), ("B", 0), ("pick", 2),
+    ("pick", 3), ("w", 0), ("w", 1), ("gu", 0), ("A", 1), ("B", 1), ("w", 2), ("dn", 0), ("ga", 1),
+    ("A", 2), ("B", 2), ("red", 0), ("gb", 1), ("dn", 1), ("ga", 2), ("red", 1), ("gb", 2),
+    ("A", 3), ("B", 3), ("dn", 2), ("ga", 3), ("red", 2), ("gb", 3), ("dn", 3), ("fin", 0),
+    ("red", 3), ("fin", 1), ("fin", 2), ("fin", 3), ("rel", 0), ("rel", 1), ("rel", 2), ("rel", 3),
+    ("mix", 0), ("mix", 1), ("mix", 2), ("mix", 3),
 )
 
 
@@ -436,9 +471,9 @@
     tok_dev, width = tokens.shape
     d, ff = w_gate.shape[1:]
     count = chosen.shape[1]
-    step = 32 * sum(SHARES)
-    rows = -(-count // step) * step
-    sizes = tuple(rows // sum(SHARES) * share for share in SHARES)
+    rows = -(-count // 8) * 8
+    size = -(-count // (32 * len(SHARES))) * 32
+    sizes = (size,) * (len(SHARES) - 1) + (rows - size * (len(SHARES) - 1),)
     largest = max(sizes)
     f32, bf16 = jnp.float32, jnp.bfloat16
     vmem = pl.BlockSpec(memory_space=pltpu.VMEM)

time: 43.2 us -> 41.4 us (0.958)
  Pallas kernels: 42.4 us -> 40.6 us
    pallas_call x1, Pallas kernels: 42.4 us -> 40.6 us  [fused(): pl.pallas_call(functools.partial(kernel, ep, tp, sizes), out_shape=pltpu....]
where the time goes in v2:
time: 41.4 us; the launch traced here: 41.2 us
  Pallas kernels  40.6 us (98%)
  local copies, waits for them, and re-layouts  0.64 us (2%)
    pallas_call x1, Pallas kernels, fused(): pl.pallas_call(functools.partial(kernel, ep, tp, sizes), out_shape=pltpu....  40.6 us

profile of v2, /device:TPU:0, one launch (start us, length us, event | category | flops | bytes accessed | tf_op | source)
XLA Modules:
  0.0 41.2 jit_solution(14253548434952691370)
XLA Ops:
  0.0 40.6 %shard_map.73 = bf16[168,256]{1,0:T(8,128)(2,1)S(1)} custom-call(bf16[168,256]{1,0:T(8,128)(2,1)} %tok_hbm.1, f32[1,256]{1,0:T(1,128)} %bitcast.1, s32[1,504]{1,0:T(1,128)} %chosen_hbm.1, f32[1,504]{1,0:T(1,128)} %aff_hbm.1, bf16[1,2048,1024]{2,1,0:T(8,128)(2,1)} %wg_hbm.1, bf16[1,2048,1024]{2,1,0:T(8,128)(2,1)} %wu_hbm.1, bf16[1,1024,2048]{2,1,0:T(8,128)(2,1)} %wd_hbm.1), custom_call_target="tpu_custom_call" | custom-call | tf_op jit(solution)/shard_map/pallas_call | solution.py:482
  40.6 0.6 %copy.9 = bf16[168,256]{1,0:T(8,128)(2,1)} copy(bf16[168,256]{1,0:T(8,128)(2,1)S(1)} %shard_map.73) | data formatting | bytes 172032

commit v3 on v2

--- a/solution.py
+++ b/solution.py
@@ -408,7 +408,7 @@
                     back[k, rows_c, :] = jnp.dot(
                         hots[k], weighted[low : ends[c], :], preferred_element_type=f32
                     ).astype(bf16)
-                for k in hops:
+                for k in farthest_first():
                     back_copy(c, k).start()
 
     def back_copy(c, k):

time: 41.4 us -> 41.3 us (level)
  no operation moved by 1% of the time
where the time goes in v3:
time: 41.3 us; the launch traced here: 41.1 us
  Pallas kernels  40.5 us (98%)
  local copies, waits for them, and re-layouts  0.64 us (2%)
    pallas_call x1, Pallas kernels, fused(): pl.pallas_call(functools.partial(kernel, ep, tp, sizes), out_shape=pltpu....  40.5 us

profile of v3, /device:TPU:0, one launch (start us, length us, event | category | flops | bytes accessed | tf_op | source)
XLA Modules:
  0.0 41.1 jit_solution(8622107528177466917)
XLA Ops:
  0.0 40.5 %shard_map.73 = bf16[168,256]{1,0:T(8,128)(2,1)S(1)} custom-call(bf16[168,256]{1,0:T(8,128)(2,1)} %tok_hbm.1, f32[1,256]{1,0:T(1,128)} %bitcast.1, s32[1,504]{1,0:T(1,128)} %chosen_hbm.1, f32[1,504]{1,0:T(1,128)} %aff_hbm.1, bf16[1,2048,1024]{2,1,0:T(8,128)(2,1)} %wg_hbm.1, bf16[1,2048,1024]{2,1,0:T(8,128)(2,1)} %wu_hbm.1, bf16[1,1024,2048]{2,1,0:T(8,128)(2,1)} %wd_hbm.1), custom_call_target="tpu_custom_call" | custom-call | tf_op jit(solution)/shard_map/pallas_call | solution.py:482
  40.5 0.6 %copy.9 = bf16[168,256]{1,0:T(8,128)(2,1)} copy(bf16[168,256]{1,0:T(8,128)(2,1)S(1)} %shard_map.73) | data formatting | bytes 172032
